TPU v7x, 512 devices: a whole 4x4x16 slice. The times are simulated.
512 devices in a mesh: ep: 32 (over z, core), tp: 16 (over y, x).
Axes of the slice: x: 4, y: 4, z: 16, core: 2. Of those that a mesh axis runs over, the one named last changes fastest.
Arguments:
- conv_input: bfloat16 [1024, 65536], P('tp', 'ep'), may hold values from -6 to 6
- out_gate: bfloat16 [1024, 65536], P('tp', 'ep'), may hold values from -6 to 6
- in_gate: bfloat16 [1024, 65536], P('tp', 'ep'), may hold values from -6 to 6
- conv_taps: float32 [3, 1024], replicated, may hold values from -3.5 to 3.5
- mixer_proj: bfloat16 [1024, 2048], P(None, 'tp'), may hold values from -0.1875 to 0.1875
- token_rows: bfloat16 [8192, 2048], P('ep', 'tp'), may hold values from -4000 to 4000
- routes: int32 [8192, 2], P('ep'), may hold values from 0 to 31, as said below
- route_weights: float32 [8192, 2], P('ep'), may hold values from 0.3 to 1
- expert_gate: bfloat16 [32, 2048, 4096], P('ep', None, 'tp'), may hold values from -0.125 to 0.125
- expert_up: bfloat16 [32, 2048, 4096], P('ep', None, 'tp'), may hold values from -0.125 to 0.125
- expert_down: bfloat16 [32, 4096, 2048], P('ep', 'tp'), may hold values from -0.125 to 0.125
Outputs:
- mixed_out: bfloat16 [65536, 2048], P('ep', 'tp')
- expert_out: bfloat16 [8192, 2048], P('ep', 'tp')
Inputs may be any that keep to these rules, and one draw needn't show every extreme that they name: `routes`: in each aligned block of 256 rows, no expert is named more than 32 times and one expert, the same in every block, exactly 32 times; the two experts of a row differ.
All inputs are finite; a program needn't handle non-finite values.
Results may differ from a plain program's by a relative error of at most 0.015.
Values may be sent and summed in bfloat16 or wider, within the bound.
A program may use at most 64 MiB of HBM per device.

v0:
```python
import jax
import jax.numpy as jnp
from jax import lax
from jax.sharding import PartitionSpec as P

KERNEL = 3
EPSILON = 1e-06


def passed_along(value, axis, by):
    devices = lax.axis_size(axis)
    pairs = [(i, i + by) for i in range(devices) if 0 <= i + by < devices]
    return lax.ppermute(value, axis, pairs)


def split_up(value, dim, devices):
    before, after = (value.shape[:dim], value.shape[dim + 1 :])
    return jnp.moveaxis(value.reshape(*before, devices, -1, *after), dim, 0)


def sent_and_summed(value, axis, dim):
    blocks = split_up(value, dim, lax.axis_size(axis))
    arrived = lax.all_to_all(blocks, axis, split_axis=0, concat_axis=0, tiled=True)
    return arrived.astype(jnp.float32).sum(axis=0)


def slot_places(route_ids, capacity, experts):
    flat_ids = route_ids.reshape(-1)
    hit_table = (flat_ids[:, None] == jnp.arange(experts, dtype=jnp.int32)[None, :]).astype(
        jnp.int32
    )
    earlier = jnp.cumsum(hit_table, axis=0) - hit_table
    slot_rank = jnp.sum(earlier * hit_table, axis=1)
    return flat_ids * capacity + slot_rank


def body(
    conv_input,
    out_gate,
    in_gate,
    conv_taps,
    mixer_proj,
    token_rows,
    routes,
    route_weights,
    expert_gate,
    expert_up,
    expert_down,
):
    width_part = conv_input.shape[0]
    length = conv_input.shape[1]
    offset = lax.axis_index("tp") * width_part
    local_taps = lax.dynamic_slice_in_dim(conv_taps, offset, width_part, 1)
    z_rows = (conv_input.astype(jnp.float32) * in_gate.astype(jnp.float32)).astype(jnp.bfloat16)
    rim_rows = passed_along(z_rows[:, length - (KERNEL - 1) :], "ep", 1)
    longer = jnp.concatenate([rim_rows, z_rows], axis=1).astype(jnp.float32)
    conv_sum = jnp.zeros(z_rows.shape, jnp.float32)
    for lag_index in range(KERNEL):
        begin = KERNEL - 1 - lag_index
        conv_sum = conv_sum + local_taps[lag_index][:, None] * longer[:, begin : begin + length]
    gated = (out_gate.astype(jnp.float32) * conv_sum).astype(jnp.bfloat16)
    mixed_sum = lax.dot_general(
        lax.all_gather(gated, "tp", axis=0, tiled=True),
        mixer_proj,
        (((0,), (0,)), ((), ())),
        preferred_element_type=jnp.float32,
    )
    mixed_out = mixed_sum.astype(jnp.bfloat16)
    experts = lax.axis_size("ep")
    rows_b = token_rows.shape[0]
    cols_part = token_rows.shape[1]
    capacity = 4 * rows_b // experts
    slot_total = experts * capacity
    places = slot_places(routes, capacity, experts)
    sources = jnp.arange(2 * rows_b, dtype=jnp.int32) // 2
    gate_weight = expert_gate[0]
    up_weight = expert_up[0]
    down_weight = expert_down[0]
    feature_count = cols_part * lax.axis_size("tp")
    buffer = jnp.zeros((slot_total, cols_part), jnp.bfloat16).at[places].set(token_rows[sources])
    arrived = lax.all_to_all(
        buffer.reshape(experts, capacity, cols_part), "ep", split_axis=0, concat_axis=0, tiled=True
    )
    arrived = arrived.reshape(slot_total, cols_part)
    part_in = lax.all_gather(arrived, "tp", axis=1, tiled=True)
    gate_sum = jnp.dot(part_in, gate_weight, preferred_element_type=jnp.float32)
    up_sum = jnp.dot(part_in, up_weight, preferred_element_type=jnp.float32)
    squares = jnp.sum(jnp.square(part_in.astype(jnp.float32)), axis=1)
    row_scale = lax.rsqrt(squares / feature_count + EPSILON)[:, None]
    hidden = (jax.nn.silu(row_scale * gate_sum) * (row_scale * up_sum)).astype(jnp.bfloat16)
    summed = sent_and_summed(
        lax.dot_general(
            down_weight, hidden, (((0,), (1,)), ((), ())), preferred_element_type=jnp.float32
        ).astype(jnp.bfloat16),
        "tp",
        0,
    )
    expert_rows = summed.astype(jnp.bfloat16).reshape(cols_part, experts, capacity)
    returned = lax.all_to_all(expert_rows, "ep", split_axis=1, concat_axis=1, tiled=True).reshape(
        cols_part, slot_total
    )
    picked = returned[:, places].astype(jnp.float32).reshape(cols_part, rows_b, 2)
    combined = jnp.sum(picked * route_weights[None, :, :], axis=2)
    expert_out = combined.T.astype(jnp.bfloat16)
    return (mixed_out, expert_out)


def solution(mesh):
    return jax.shard_map(
        body,
        mesh=mesh,
        in_specs=(
            P("tp", "ep"),
            P("tp", "ep"),
            P("tp", "ep"),
            P(),
            P(None, "tp"),
            P("ep", "tp"),
            P("ep", None),
            P("ep", None),
            P("ep", None, "tp"),
            P("ep", None, "tp"),
            P("ep", "tp", None),
        ),
        out_specs=(P("ep", "tp"), P("ep", "tp")),
        check_vma=False,
    )
```

profile of v0, /device:TPU:1, one launch (start us, length us, event | category | flops | bytes accessed | tf_op | source)
XLA Modules:
  0.0 242.8 jit_solution(143505425020026601)
XLA Ops:
  7.2 0.0 copy-start
  7.2 0.0 all-gather.5.cloned.1.call-start
  7.2 0.9 copy.26
  8.1 0.1 eq.29
  8.3 0.1 eq.25
  8.4 0.7 broadcast_multiply_fusion
  9.1 1.2 reduce-window.6
  10.3 0.2 slice_reduce_fusion
  10.6 0.1 copy.25
  10.7 0.1 mul.101
  10.9 0.1 fusion.18
  11.0 4.9 %scatter_custom_fusion = bf16[1024,128]{1,0:T(8,128)(2,1)S(1)} fusion(s32[512]{0:T(512)S(1)} %bitcast.65, bf16[256,128]{1,0:T(8,128)(2,1)} %param.16, s32[1024]{0:T(1024)S(1)} %pad_clamp_fusion.1, bf16[]{:T(256)} %constant.39.clone.1), kind=kCustom, calls=%fused_computation.26 | custom fusion | bytes 262656 | tf_op jit(solution)/shard_map/scatter | solution.py:80
  15.9 38.9 %all_to_all.15 = bf16[32,32,128]{2,1,0:T(8,128)(2,1)} all-to-all(bf16[32,32,128]{2,1,0:T(8,128)(2,1)S(1)} %bitcast.63), channel_id=1, replica_groups=mesh['ep'=32,'tp'=16] {'ep'}, dimensions={0} | all-to-all | bytes 524288 | tf_op jit(solution)/shard_map/all_to_all | solution.py:81
  54.8 0.0 copy-start.3
  54.8 0.0 all-gather.5.cloned.1.call-update
  54.8 0.0 all-gather.3.cloned.1.call-start
  54.9 1.2 multiply_convert_fusion
  56.0 0.1 slice.40
  56.1 2.2 collective-permute-start
  58.4 0.8 constant_dynamic-slice_fusion
  59.1 0.1 collective-permute-done
  59.2 0.1 maximum_convert_fusion
  59.4 2.0 fusion.9
  61.4 0.0 all-gather.3.cloned.1.call-update
  61.4 55.6 %all-gather.5.cloned.1.call-done = bf16[1024,2048]{1,0:T(8,128)(2,1)} async-done(((bf16[1024,128]{1,0:T(8,128)(2,1)}), bf16[1024,2048]{1,0:T(8,128)(2,1)}) %all-gather.5.cloned.1.call-update) | async-done | bytes 4194320 | tf_op jit(solution)/shard_map/all_gather | solution.py:85
  117.1 0.0 copy-start.1
  117.1 3.2 %multiply_reduce_fusion = f32[1024]{0:T(1024)S(1)} fusion(bf16[1024,2048]{1,0:T(8,128)(2,1)} %all-gather.5.cloned.1.call-done), kind=kLoop, calls=%fused_computation.3 | loop fusion | flops 6290432 | bytes 4198400 | tf_op jit(solution)/shard_map/reduce_sum | solution.py:88
  120.3 0.0 copy-start.4
  120.3 0.0 copy-done.3
  120.3 0.2 copy-done.1
  120.5 2.3 convolution_multiply_fusion.1
  122.8 0.0 copy-done
  122.8 0.0 copy-done.4
  122.8 8.8 %convert_bitcast_fusion = bf16[128,16,8,128]{3,2,1,0:T(8,128)(2,1)} fusion(bf16[1,256,2048]{2,1,0:T(8,128)(2,1)S(1)} %copy-done, bf16[1024,2048]{1,0:T(8,128)(2,1)} %all-gather.5.cloned.1.call-done, bf16[1,2048,256]{2,1,0:T(8,128)(2,1)S(1)} %copy-done.4, f32[1024,256]{1,0:T(8,128)} %convolution_multiply_fusion.1, f32[1024]{0:T(1024)S(1)} %add_rsqrt_fusion), kind=kOutput, calls=%fused_computation.5 | convolution fusion | flops 2151415808 | bytes 11538432 | tf_op jit(solution)/shard_map/dot_general | solution.py:92
  131.6 3.3 %copy.35 = bf16[128,16,8,128]{3,2,0,1:T(8,128)(2,1)S(1)} copy(bf16[128,16,8,128]{3,2,1,0:T(8,128)(2,1)} %convert_bitcast_fusion) | data formatting | bytes 8388608 | tf_op jit(solution)/shard_map/reshape | solution.py:18
  134.9 58.8 %all_to_all.16 = bf16[16,128,1024]{1,2,0:T(8,128)(2,1)} all-to-all(bf16[16,128,1024]{1,2,0:T(8,128)(2,1)S(1)} %bitcast.59), channel_id=1, replica_groups=mesh['ep'=32,'tp'=16] {'tp'}, dimensions={0} | all-to-all | bytes 8388608 | tf_op jit(solution)/shard_map/all_to_all | solution.py:23
  193.7 0.0 copy-start.2
  193.7 0.0 copy-start.5
  193.7 3.9 %reduce_sum.44 = bf16[128,1024]{0,1:T(8,128)(2,1)} reduce(bf16[16,128,1024]{1,2,0:T(8,128)(2,1)} %all_to_all.16, bf16[]{:T(256)} %constant.39.clone.1), dimensions={0}, to_apply=%region_5.6 | reduce | flops 1966080 | bytes 4456450 | tf_op jit(solution)/shard_map/reduce_sum | solution.py:24
  197.6 13.7 %all-to-all-start.2 = ((bf16[128,32,32]{0,2,1:T(8,128)(2,1)}), bf16[128,32,32]{0,2,1:T(8,128)(2,1)S(1)}, u32[]{:S(2)}, u32[]{:S(2)}) async-start(bf16[128,32,32]{0,2,1:T(8,128)(2,1)} %bitcast.13), calls=%async_computation.2 | async-start | bytes 524288 | tf_op jit(solution)/shard_map/all_to_all | solution.py:99
  211.3 0.0 copy-done.2
  211.3 0.1 copy.30
  211.5 3.2 %all-gather.3.cloned.1.call-done = bf16[1024,2048]{1,0:T(8,128)(2,1)} async-done(((bf16[64,2048]{1,0:T(8,128)(2,1)}), bf16[1024,2048]{1,0:T(8,128)(2,1)}) %all-gather.3.cloned.1.call-update) | async-done | bytes 4194320 | tf_op jit(solution)/shard_map/all_gather | solution.py:63
  214.7 0.0 copy-done.5
  214.7 4.3 %convolution_convert_fusion = bf16[2048,128]{1,0:T(8,128)(2,1)} fusion(bf16[1024,2048]{1,0:T(8,128)(2,1)} %all-gather.3.cloned.1.call-done, bf16[1024,128]{1,0:T(8,128)(2,1)S(1)} %copy-done.5), kind=kOutput, calls=%fused_computation.6 | convolution fusion | flops 537133056 | bytes 4980736 | tf_op jit(solution)/shard_map/dot_general | solution.py:62
  219.0 14.6 %all-to-all-done.2 = bf16[128,32,32]{0,2,1:T(8,128)(2,1)S(1)} async-done(((bf16[128,32,32]{0,2,1:T(8,128)(2,1)}), bf16[128,32,32]{0,2,1:T(8,128)(2,1)S(1)}, u32[]{:S(2)}, u32[]{:S(2)}) %all-to-all-start.2) | async-done | bytes 262176 | tf_op jit(solution)/shard_map/all_to_all | solution.py:99
  233.6 1.3 gather_fusion
  234.9 1.0 multiply_reduce_fusion.1
  (10 shorter events, 0.1 us)
Async XLA Ops:
  7.2 115.7 %copy-start = (bf16[1,256,2048]{2,1,0:T(8,128)(2,1)S(1)}, bf16[1,256,2048]{2,1,0:T(8,128)(2,1)}, u32[]{:S(2)}) copy-start(bf16[1,256,2048]{2,1,0:T(8,128)(2,1)} %param.21) | copy-start | bytes 3145732
  7.2 109.9 %all-gather.5.cloned.1.call-start = ((), (), s32[]{:S(2)}) async-start(), calls=%async_computation.4 | async-start | bytes 4456448 | tf_op jit(solution)/shard_map/all_gather | solution.py:85
  54.8 65.5 %copy-start.3 = (bf16[1,2048,256]{2,1,0:T(8,128)(2,1)S(1)}, bf16[1,2048,256]{2,1,0:T(8,128)(2,1)}, u32[]{:S(2)}) copy-start(bf16[1,2048,256]{2,1,0:T(8,128)(2,1)} %param.19) | copy-start | bytes 3145732
  54.8 159.8 %all-gather.3.cloned.1.call-start = ((), (), s32[]{:S(2)}) async-start(), calls=%async_computation.3 | async-start | bytes 4456448 | tf_op jit(solution)/shard_map/all_gather | solution.py:63
  56.1 3.1 %collective-permute-start = (bf16[64,2]{1,0:T(8,128)(2,1)S(1)}, bf16[64,2]{1,0:T(8,128)(2,1)S(1)}, u32[]{:S(2)}, u32[]{:S(2)}) collective-permute-start(bf16[64,2]{1,0:T(8,128)(2,1)S(1)} %slice.40), channel_id=1, source_target_pairs={{0,16},{16,32},{32,48},{48,64},{64,80},{80,96},{96,112},{112,128},... | collective-permute-start | bytes 776 | tf_op jit(solution)/shard_map/ppermute | solution.py:13
  117.1 3.4 %copy-start.1 = (bf16[1024,2048]{1,0:T(8,128)(2,1)S(1)}, bf16[1024,2048]{1,0:T(8,128)(2,1)}, u32[]{:S(2)}) copy-start(bf16[1024,2048]{1,0:T(8,128)(2,1)} %all-gather.5.cloned.1.call-done) | copy-start | bytes 12582916
  120.3 2.5 %copy-start.4 = (bf16[1,2048,256]{2,1,0:T(8,128)(2,1)S(1)}, bf16[1,2048,256]{2,1,0:T(8,128)(2,1)}, u32[]{:S(2)}) copy-start(bf16[1,2048,256]{2,1,0:T(8,128)(2,1)} %param.20) | copy-start | bytes 3145732
  193.7 17.6 %copy-start.2 = (f32[256,2]{0,1:T(2,128)S(1)}, f32[256,2]{0,1:T(2,128)}, u32[]{:S(2)}) copy-start(f32[256,2]{0,1:T(2,128)} %param.18) | copy-start | bytes 6148
  193.7 21.0 %copy-start.5 = (bf16[1024,128]{1,0:T(8,128)(2,1)S(1)}, bf16[1024,128]{1,0:T(8,128)(2,1)}, u32[]{:S(2)}) copy-start(bf16[1024,128]{1,0:T(8,128)(2,1)} %param.15) | copy-start | bytes 786436
  197.6 35.9 %all-to-all-start.2 = ((bf16[128,32,32]{0,2,1:T(8,128)(2,1)}), bf16[128,32,32]{0,2,1:T(8,128)(2,1)S(1)}, u32[]{:S(2)}, u32[]{:S(2)}) async-start(bf16[128,32,32]{0,2,1:T(8,128)(2,1)} %bitcast.13), calls=%async_computation.2 | async-start | bytes 524288 | tf_op jit(solution)/shard_map/all_to_all | solution.py:99
Sparse Core Ops, SparseCore 0:
  54.9 62.0 all-gather.4
  120.6 93.9 all-gather.2
where the time goes:
time: 243 us
  blocking collectives  97.7 us (40%)
  waiting for transfers between devices  73.6 us (30%)
  starting transfers between devices  16 us (7%)
  matrix products  15.4 us (6%)
  between operations  14.2 us (6%)
  other arithmetic  13.6 us (6%)
  local copies, waits for them, and re-layouts  12.4 us (5%)
    all_to_all x1, blocking collectives, sent_and_summed(): lax.all_to_all(blocks, axis, split_axis=0, concat_axis=0, tiled=True)  58.8 us
    all_gather x1, waiting for transfers between devices, body(): part_in = lax.all_gather(arrived, 'tp', axis=1, tiled=True)  55.6 us
    all_to_all x1, blocking collectives, body(): lax.all_to_all(buffer.reshape(experts, capacity, cols_part), 'ep', split_...  38.9 us
    all_to_all x1, waiting for transfers between devices, body(): lax.all_to_all(expert_rows, 'ep', split_axis=1, concat_axis=1, tiled=True)  14.6 us
    all_to_all x1, starting transfers between devices, body(): lax.all_to_all(expert_rows, 'ep', split_axis=1, concat_axis=1, tiled=True)  13.7 us
    dot_general x1, matrix products, body(): lax.dot_general(down_weight, hidden, (((0,), (1,)), ((), ())), preferred_...  8.82 us
    scatter x1, local copies, waits for them, and re-layouts, body(): jnp.zeros((slot_total, cols_part), jnp.bfloat16).at[places]  4.9 us
  transfers between devices with their start and end apart: 4, of which 4 were waited for; matrix products, arithmetic and copies ran while one was open for 12% of the time, Pallas kernels for 0%

commit v1 on v0

--- a/solution.py
+++ b/solution.py
@@ -82,7 +82,8 @@
         buffer.reshape(experts, capacity, cols_part), "ep", split_axis=0, concat_axis=0, tiled=True
     )
     arrived = arrived.reshape(slot_total, cols_part)
-    part_in = lax.all_gather(arrived, "tp", axis=1, tiled=True)
+    outgoing = jnp.stack([arrived] * lax.axis_size("tp"))
+    part_in = jnp.concatenate(lax.all_to_all(outgoing, "tp", 0, 0), axis=1)
     gate_sum = jnp.dot(part_in, gate_weight, preferred_element_type=jnp.float32)
     up_sum = jnp.dot(part_in, up_weight, preferred_element_type=jnp.float32)
     squares = jnp.sum(jnp.square(part_in.astype(jnp.float32)), axis=1)

time: 243 us -> 251 us (1.033)
  starting transfers between devices: 16 us -> 22.4 us
  blocking collectives: 97.7 us -> 92.7 us
  waiting for transfers between devices: 73.6 us -> 77 us
  matrix products: 15.4 us -> 18 us
    all_to_all x0 -> x1, waiting for transfers between devices: none -> 59.2 us  [body(): part_in = jnp.concatenate(lax.all_to_all(outgoing, 'tp', 0, 0), axis=1)]
    all_gather x1 -> x0, waiting for transfers between devices: 55.6 us -> none  [body(): part_in = lax.all_gather(arrived, 'tp', axis=1, tiled=True)]
    all_to_all x0 -> x1, starting transfers between devices: none -> 6.94 us  [body(): part_in = jnp.concatenate(lax.all_to_all(outgoing, 'tp', 0, 0), axis=1)]
    all_to_all x1, blocking collectives: 58.8 us -> 53.9 us  [sent_and_summed(): lax.all_to_all(blocks, axis, split_axis=0, concat_axis=0, tiled=True)]
    all_gather x1, waiting for transfers between devices: 3.18 us -> 0.02 us  [body(): lax.all_gather(gated, 'tp', axis=0, tiled=True)]
    all_to_all x1, waiting for transfers between devices: 14.6 us -> 17.8 us  [body(): lax.all_to_all(expert_rows, 'ep', split_axis=1, concat_axis=1, tiled=True)]
    another operation x1 -> x3, local copies, waits for them, and re-layouts: 0.01 us -> 2.66 us  [the longest x2 2.66 us: body(): outgoing = jnp.stack([arrived] * lax.axis_size('tp'))]
  transfers between devices with their start and end apart: 4 -> 4, of which waited for: 4 -> 2; matrix products, arithmetic and copies ran while one was open for 12% -> 12% of each run, Pallas kernels for 0% -> 0%
where the time goes in v1:
time: 251 us; the launch traced here: 250 us
  blocking collectives  92.7 us (37%)
  waiting for transfers between devices  77 us (31%)
  starting transfers between devices  22.4 us (9%)
  matrix products  18 us (7%)
  local copies, waits for them, and re-layouts  14.9 us (6%)
  between operations  14.3 us (6%)
  other arithmetic  11.1 us (4%)
    all_to_all x1, waiting for transfers between devices, body(): part_in = jnp.concatenate(lax.all_to_all(outgoing, 'tp', 0, 0), axis=1)  59.2 us
    all_to_all x1, blocking collectives, sent_and_summed(): lax.all_to_all(blocks, axis, split_axis=0, concat_axis=0, tiled=True)  53.9 us
    all_to_all x1, blocking collectives, body(): lax.all_to_all(buffer.reshape(experts, capacity, cols_part), 'ep', split_...  38.8 us
    all_to_all x1, waiting for transfers between devices, body(): lax.all_to_all(expert_rows, 'ep', split_axis=1, concat_axis=1, tiled=True)  17.8 us
    all_to_all x1, starting transfers between devices, body(): lax.all_to_all(expert_rows, 'ep', split_axis=1, concat_axis=1, tiled=True)  12.6 us
    dot_general x1, matrix products, body(): lax.dot_general(down_weight, hidden, (((0,), (1,)), ((), ())), preferred_...  9.14 us
    all_to_all x1, starting transfers between devices, body(): part_in = jnp.concatenate(lax.all_to_all(outgoing, 'tp', 0, 0), axis=1)  6.94 us
  transfers between devices with their start and end apart: 4, of which 2 were waited for; matrix products, arithmetic and copies ran while one was open for 12% of the time, Pallas kernels for 0%

profile of v1, /device:TPU:1, one launch (start us, length us, event | category | flops | bytes accessed | tf_op | source)
XLA Modules:
  0.0 250.4 jit_solution(8188873265201765081)
XLA Ops:
  7.2 0.0 copy-start
  7.2 0.9 copy.26
  8.1 0.1 eq.29
  8.2 0.1 eq.25
  8.4 0.7 broadcast_multiply_fusion
  9.1 1.2 reduce-window.6
  10.3 0.2 slice_reduce_fusion
  10.5 0.1 copy.25
  10.7 0.1 mul.101
  10.8 0.1 fusion.18
  10.9 4.9 %scatter_custom_fusion = bf16[1024,128]{1,0:T(8,128)(2,1)S(1)} fusion(s32[512]{0:T(512)S(1)} %bitcast.69, bf16[256,128]{1,0:T(8,128)(2,1)} %param.16, s32[1024]{0:T(1024)S(1)} %pad_clamp_fusion.1, bf16[]{:T(256)} %constant.39.clone.1), kind=kCustom, calls=%fused_computation.26 | custom fusion | bytes 262656 | tf_op jit(solution)/shard_map/scatter | solution.py:80
  15.9 38.8 %all_to_all.20 = bf16[32,32,128]{2,1,0:T(8,128)(2,1)S(1)} all-to-all(bf16[32,32,128]{2,1,0:T(8,128)(2,1)S(1)} %bitcast.66), channel_id=1, replica_groups=mesh['ep'=32,'tp'=16] {'ep'}, dimensions={0} | all-to-all | bytes 524288 | tf_op jit(solution)/shard_map/all_to_all | solution.py:81
  54.6 0.1 copy.29
  54.8 2.5 %stack.3 = bf16[16,1024,128]{1,2,0:T(8,128)(2,1)} broadcast(bf16[1024,128]{0,1:T(8,128)(2,1)S(1)} %copy.29), dimensions={1,2} | broadcast | bytes 4456448 | tf_op jit(solution)/shard_map/stack | solution.py:85
  57.3 0.0 copy-start.1
  57.3 0.0 copy-start.2
  57.3 6.9 %all-to-all-start.1 = ((bf16[16,1024,128]{1,2,0:T(8,128)(2,1)}), bf16[16,1024,128]{1,2,0:T(8,128)(2,1)}, u32[]{:S(2)}, u32[]{:S(2)}) async-start(bf16[16,1024,128]{1,2,0:T(8,128)(2,1)} %stack.3), calls=%async_computation.1 | async-start | bytes 8388608 | tf_op jit(solution)/shard_map/all_to_all | solution.py:86
  64.3 0.0 copy-start.5
  64.3 0.0 all-gather.2.cloned.1.call-start
  64.3 0.0 copy-done.1
  64.3 0.0 copy-done.2
  64.3 0.1 multiply_convert_fusion
  64.4 0.1 slice.40
  64.5 2.8 %collective-permute-start = (bf16[64,2]{1,0:T(8,128)(2,1)S(1)}, bf16[64,2]{1,0:T(8,128)(2,1)S(1)}, u32[]{:S(2)}, u32[]{:S(2)}) collective-permute-start(bf16[64,2]{1,0:T(8,128)(2,1)S(1)} %slice.40), channel_id=1, source_target_pairs={{0,16},{16,32},{32,48},{48,64},{64,80},{80,96},{96,112},{112,128},... | collective-permute-start | bytes 776 | tf_op jit(solution)/shard_map/ppermute | solution.py:13
  67.3 0.8 constant_dynamic-slice_fusion
  68.1 0.0 collective-permute-done
  68.1 0.1 maximum_convert_fusion
  68.3 0.0 copy-done.3
  68.3 1.1 fusion.9
  69.3 0.0 all-gather.2.cloned.1.call-update
  69.4 59.2 %all-to-all-done.1 = bf16[16,1024,128]{1,2,0:T(8,128)(2,1)} async-done(((bf16[16,1024,128]{1,2,0:T(8,128)(2,1)}), bf16[16,1024,128]{1,2,0:T(8,128)(2,1)}, u32[]{:S(2)}, u32[]{:S(2)}) %all-to-all-start.1) | async-done | bytes 4194336 | tf_op jit(solution)/shard_map/all_to_all | solution.py:86
  128.6 3.1 %multiply_reduce_fusion = f32[1024]{0:T(1024)S(1)} fusion(bf16[16,1024,128]{1,2,0:T(8,128)(2,1)} %all-to-all-done.1), kind=kLoop, calls=%fused_computation.3 | loop fusion | flops 6290432 | bytes 4198400 | tf_op jit(solution)/shard_map/reduce_sum | solution.py:89
  131.7 0.0 copy-done.5
  131.7 4.6 %convolution_multiply_fusion.1 = f32[1024,256]{1,0:T(8,128)} fusion(bf16[1024,2048]{0,1:T(8,128)(2,1)} %bitcast.10, bf16[1,2048,256]{2,1,0:T(8,128)(2,1)S(1)} %copy-done.5, f32[1024]{0:T(1024)S(1)} %add_rsqrt_fusion), kind=kOutput, calls=%fused_computation.8 | convolution fusion | flops 1074003968 | bytes 6295552 | tf_op jit(solution)/shard_map/dot_general | solution.py:87
  136.2 0.0 copy-done
  136.2 9.1 %convert_bitcast_fusion = bf16[128,16,8,128]{3,2,1,0:T(8,128)(2,1)} fusion(bf16[1,256,2048]{2,1,0:T(8,128)(2,1)S(1)} %copy-done, bf16[1024,2048]{0,1:T(8,128)(2,1)} %bitcast.10, bf16[1,2048,256]{2,1,0:T(8,128)(2,1)} %param.20, f32[1024,256]{1,0:T(8,128)} %convolution_multiply_fusion.1, f32[1024]{0:T(1024)S(1)} %add_rsqrt_fusion), kind=kOutput, calls=%fused_computation.5 | convolution fusion | flops 2151415808 | bytes 11538432 | tf_op jit(solution)/shard_map/dot_general | solution.py:93
  145.4 3.3 %copy.36 = bf16[128,16,8,128]{3,2,0,1:T(8,128)(2,1)S(1)} copy(bf16[128,16,8,128]{3,2,1,0:T(8,128)(2,1)} %convert_bitcast_fusion) | data formatting | bytes 8388608 | tf_op jit(solution)/shard_map/reshape | solution.py:18
  148.7 53.9 %all_to_all.21 = bf16[16,128,1024]{1,2,0:T(8,128)(2,1)} all-to-all(bf16[16,128,1024]{1,2,0:T(8,128)(2,1)S(1)} %bitcast.63), channel_id=1, replica_groups=mesh['ep'=32,'tp'=16] {'tp'}, dimensions={0} | all-to-all | bytes 8388608 | tf_op jit(solution)/shard_map/all_to_all | solution.py:23
  202.7 3.6 %reduce_sum.44 = bf16[128,1024]{0,1:T(8,128)(2,1)} reduce(bf16[16,128,1024]{1,2,0:T(8,128)(2,1)} %all_to_all.21, bf16[]{:T(256)} %constant.39.clone.1), dimensions={0}, to_apply=%region_5.6 | reduce | flops 1966080 | bytes 4456450 | tf_op jit(solution)/shard_map/reduce_sum | solution.py:24
  206.3 12.6 %all-to-all-start.3 = ((bf16[128,32,32]{0,2,1:T(8,128)(2,1)}), bf16[128,32,32]{0,2,1:T(8,128)(2,1)S(1)}, u32[]{:S(2)}, u32[]{:S(2)}) async-start(bf16[128,32,32]{0,2,1:T(8,128)(2,1)} %bitcast.16), calls=%async_computation.3 | async-start | bytes 524288 | tf_op jit(solution)/shard_map/all_to_all | solution.py:100
  218.9 0.0 copy-done.4
  218.9 0.1 copy.31
  219.1 0.0 all-gather.2.cloned.1.call-done
  219.1 0.0 copy-done.6
  219.1 4.3 %convolution_convert_fusion = bf16[2048,128]{1,0:T(8,128)(2,1)} fusion(bf16[1024,2048]{1,0:T(8,128)(2,1)} %all-gather.2.cloned.1.call-done, bf16[1024,128]{1,0:T(8,128)(2,1)S(1)} %copy-done.6), kind=kOutput, calls=%fused_computation.6 | convolution fusion | flops 537133056 | bytes 4980736 | tf_op jit(solution)/shard_map/dot_general | solution.py:62
  223.4 17.8 %all-to-all-done.3 = bf16[128,32,32]{0,2,1:T(8,128)(2,1)S(1)} async-done(((bf16[128,32,32]{0,2,1:T(8,128)(2,1)}), bf16[128,32,32]{0,2,1:T(8,128)(2,1)S(1)}, u32[]{:S(2)}, u32[]{:S(2)}) %all-to-all-start.3) | async-done | bytes 262176 | tf_op jit(solution)/shard_map/all_to_all | solution.py:100
  241.2 1.3 gather_fusion
  242.5 1.0 multiply_reduce_fusion.1
  (13 shorter events, 0.1 us)
Async XLA Ops:
  7.2 129.1 %copy-start = (bf16[1,256,2048]{2,1,0:T(8,128)(2,1)S(1)}, bf16[1,256,2048]{2,1,0:T(8,128)(2,1)}, u32[]{:S(2)}) copy-start(bf16[1,256,2048]{2,1,0:T(8,128)(2,1)} %param.21) | copy-start | bytes 3145732
  57.3 7.0 %copy-start.1 = (bf16[64,2048]{1,0:T(8,128)(2,1)S(1)}, bf16[64,2048]{1,0:T(8,128)(2,1)}, u32[]{:S(2)}) copy-start(bf16[64,2048]{1,0:T(8,128)(2,1)} %param.13) | copy-start | bytes 786436
  57.3 7.0 %copy-start.2 = (bf16[64,2048]{1,0:T(8,128)(2,1)S(1)}, bf16[64,2048]{1,0:T(8,128)(2,1)}, u32[]{:S(2)}) copy-start(bf16[64,2048]{1,0:T(8,128)(2,1)} %param.11) | copy-start | bytes 786436
  57.3 10.9 %copy-start.3 = (bf16[64,2048]{1,0:T(8,128)(2,1)S(1)}, bf16[64,2048]{1,0:T(8,128)(2,1)}, u32[]{:S(2)}) copy-start(bf16[64,2048]{1,0:T(8,128)(2,1)} %param.12) | copy-start | bytes 786436
  57.3 71.2 %all-to-all-start.1 = ((bf16[16,1024,128]{1,2,0:T(8,128)(2,1)}), bf16[16,1024,128]{1,2,0:T(8,128)(2,1)}, u32[]{:S(2)}, u32[]{:S(2)}) async-start(bf16[16,1024,128]{1,2,0:T(8,128)(2,1)} %stack.3), calls=%async_computation.1 | async-start | bytes 8388608 | tf_op jit(solution)/shard_map/all_to_all | solution.py:86
  64.3 67.4 %copy-start.5 = (bf16[1,2048,256]{2,1,0:T(8,128)(2,1)S(1)}, bf16[1,2048,256]{2,1,0:T(8,128)(2,1)}, u32[]{:S(2)}) copy-start(bf16[1,2048,256]{2,1,0:T(8,128)(2,1)} %param.19) | copy-start | bytes 3145732
  64.3 154.8 %all-gather.2.cloned.1.call-start = ((), (), s32[]{:S(2)}) async-start(), calls=%async_computation.4 | async-start | bytes 4456448 | tf_op jit(solution)/shard_map/all_gather | solution.py:63
  64.5 3.6 %collective-permute-start = (bf16[64,2]{1,0:T(8,128)(2,1)S(1)}, bf16[64,2]{1,0:T(8,128)(2,1)S(1)}, u32[]{:S(2)}, u32[]{:S(2)}) collective-permute-start(bf16[64,2]{1,0:T(8,128)(2,1)S(1)} %slice.40), channel_id=1, source_target_pairs={{0,16},{16,32},{32,48},{48,64},{64,80},{80,96},{96,112},{112,128},... | collective-permute-start | bytes 776 | tf_op jit(solution)/shard_map/ppermute | solution.py:13
  202.7 16.2 %copy-start.4 = (f32[256,2]{0,1:T(2,128)S(1)}, f32[256,2]{0,1:T(2,128)}, u32[]{:S(2)}) copy-start(f32[256,2]{0,1:T(2,128)} %param.18) | copy-start | bytes 6148
  202.7 16.4 %copy-start.6 = (bf16[1024,128]{1,0:T(8,128)(2,1)S(1)}, bf16[1024,128]{1,0:T(8,128)(2,1)}, u32[]{:S(2)}) copy-start(bf16[1024,128]{1,0:T(8,128)(2,1)} %param.15) | copy-start | bytes 786436
  206.3 34.9 %all-to-all-start.3 = ((bf16[128,32,32]{0,2,1:T(8,128)(2,1)}), bf16[128,32,32]{0,2,1:T(8,128)(2,1)S(1)}, u32[]{:S(2)}, u32[]{:S(2)}) async-start(bf16[128,32,32]{0,2,1:T(8,128)(2,1)} %bitcast.16), calls=%async_computation.3 | async-start | bytes 524288 | tf_op jit(solution)/shard_map/all_to_all | solution.py:100
Sparse Core Ops, SparseCore 0:
  69.5 85.3 all-gather.1
